TPU v7x, 32 devices: a whole 2x2x4 slice. The times are simulated.
32 devices in a mesh: sp: 4 (over z), fs: 4 (over y, x), tp: 2 (over core).
Axes of the slice: x: 2, y: 2, z: 4, core: 2. Of those that a mesh axis runs over, the one named last changes fastest.
Arguments:
- activations: bfloat16 [4, 1024, 2048], P('fs', 'sp'), may hold values from -600 to 600
- norm_gain: float32 [2048], replicated, may hold values from 0.1 to 1.9
- w_conv_gate: bfloat16 [2048, 1024], P('sp', ('fs', 'tp')), may hold values from -0.125 to 0.125
- w_conv_mult: bfloat16 [2048, 1024], P('sp', ('fs', 'tp')), may hold values from -0.125 to 0.125
- w_conv_in: bfloat16 [2048, 1024], P('sp', ('fs', 'tp')), may hold values from -0.125 to 0.125
- conv_taps: float32 [3, 1024], replicated, may hold values from -3.5 to 3.5
- w_query: bfloat16 [2048, 1024], P('sp', ('fs', 'tp')), may hold values from -0.125 to 0.125
- w_key: bfloat16 [2048, 1024], P('sp', ('fs', 'tp')), may hold values from -0.125 to 0.125
- w_value: bfloat16 [2048, 1024], P('sp', ('fs', 'tp')), may hold values from -0.125 to 0.125
- w_input_gate: bfloat16 [2048, 8], replicated, may hold values from -0.125 to 0.125
- w_forget_gate: bfloat16 [2048, 8], replicated, may hold values from -0.125 to 0.125
- gate_bias: float32 [2, 8], replicated, may hold values from -1 to 120
- decay_shift: float32 [4, 1024, 8], P(None, 'sp'), may hold values from -2 to 0, as said below
- head_gain: float32 [1024], replicated, may hold values from 0.1 to 1.9
- w_out_conv: bfloat16 [1024, 2048], P(('fs', 'tp'), 'sp'), may hold values from -0.125 to 0.125
- w_out_mem: bfloat16 [1024, 2048], P(('fs', 'tp'), 'sp'), may hold values from -0.125 to 0.125
Outputs:
- output: bfloat16 [4, 1024, 2048], P('fs', ('sp', 'tp'))
Inputs may be any that keep to these rules, and one draw needn't show every extreme that they name: `decay_shift`: never positive.
All inputs are finite; a program needn't handle non-finite values.
Results may differ from a plain program's by a relative error of at most 0.015.
Values may be sent and summed in bfloat16 or wider, within the bound.
A program may use at most 64 MiB of HBM per device.

v0:
```python
import jax
import jax.numpy as jnp
from jax import lax
from jax.sharding import PartitionSpec as P

MEMORY_HEADS = 8
HEAD_DIM = 128
BLOCK = 64


EPSILON = 1e-06
FAR_BELOW = -1e30
HIGHEST_PRECISION = lax.Precision.HIGHEST


def prefix(value, axis, join, neutral):
    count, mine = (lax.axis_size(axis), lax.axis_index(axis))
    pieces = jax.tree.map(lambda part: lax.all_gather(part, axis), value)
    subtotal = jax.tree.map(
        lambda part, zero: jnp.full_like(part, 0) + jnp.asarray(zero, part.dtype), value, neutral
    )

    def lap(position, subtotal):
        longer = join(subtotal, jax.tree.map(lambda part: part[position], pieces))
        return jax.tree.map(lambda new, old: jnp.where(position < mine, new, old), longer, subtotal)

    return lax.fori_loop(0, count - 1, lap, subtotal)


def from_behind(array, axis, by):
    peers = lax.axis_size(axis)
    pairs = [(i, i + by) for i in range(peers) if 0 <= i + by < peers]
    return lax.ppermute(array, axis, pairs)


def combine_states(earlier, later):
    total_one, peak_one, state_one = earlier
    total_two, peak_two, state_two = later
    peak_new = jnp.maximum(total_two + peak_one, peak_two)
    scale_old = jnp.exp(total_two + peak_one - peak_new)
    scale_new = jnp.exp(peak_two - peak_new)
    return (
        total_one + total_two,
        peak_new,
        scale_old[..., None, None] * state_one + scale_new[..., None, None] * state_two,
    )


def head_rows(values, seq_count, heads_here):
    tokens = values.shape[1]
    split_heads = values.reshape(seq_count, tokens, heads_here, HEAD_DIM).transpose(0, 2, 1, 3)
    return split_heads.reshape(seq_count * heads_here, tokens, HEAD_DIM).astype(jnp.float32)


def gate_rows(values, seq_count, heads_here):
    tokens = values.shape[1]
    return values.transpose(0, 2, 1).reshape(seq_count * heads_here, tokens)


def memory_cell(query_rows, key_rows, value_rows, entry_gate, log_forget):
    members = query_rows.shape[0]
    tokens = query_rows.shape[1]
    head_width = query_rows.shape[2]
    nblocks = tokens // BLOCK
    block_shape = (members, nblocks, BLOCK, head_width)
    query_blocks = query_rows.reshape(block_shape)
    key_blocks = key_rows.reshape(block_shape) * head_width ** (-0.5)
    value_blocks = value_rows.reshape(block_shape)
    entry_blocks = entry_gate.reshape(members, nblocks, BLOCK)
    forget_sums = jnp.cumsum(log_forget.reshape(members, nblocks, BLOCK), axis=-1)
    block_total = forget_sums[..., -1]
    local_logs = block_total[..., None] - forget_sums + entry_blocks
    local_peak = jnp.max(local_logs, axis=-1)
    local_weights = jnp.exp(local_logs - local_peak[..., None])
    local_state = jnp.einsum(
        "bclv,bclk->bcvk",
        local_weights[..., None] * value_blocks,
        key_blocks,
        precision=HIGHEST_PRECISION,
    )

    def advance(running, block_item):
        return (combine_states(running, block_item), running)

    zero_sums = jnp.zeros((members,), jnp.float32)
    low_peaks = jnp.full((members,), FAR_BELOW, jnp.float32)
    zero_states = jnp.zeros((members, head_width, head_width), jnp.float32)
    block_items = (
        jnp.moveaxis(block_total, 1, 0),
        jnp.moveaxis(local_peak, 1, 0),
        jnp.moveaxis(local_state, 1, 0),
    )
    device_total, inner_states = lax.scan(advance, (zero_sums, low_peaks, zero_states), block_items)
    inner_states = tuple((jnp.moveaxis(tensor, 0, 1) for tensor in inner_states))
    total_sum, total_peak, total_state = device_total
    before = prefix(
        (total_sum, total_peak, total_state),
        "sp",
        combine_states,
        (zero_sums, low_peaks, zero_states),
    )
    opening = combine_states((zero_sums, zero_sums, zero_states), before)
    opening = tuple((tensor[:, None] for tensor in opening))
    _, prior_peak, prior_state = combine_states(opening, inner_states)
    positions = jnp.arange(BLOCK)
    causal_mask = positions[:, None] >= positions[None, :]
    pair_logs = jnp.where(
        causal_mask,
        forget_sums[..., :, None] - forget_sums[..., None, :] + entry_blocks[..., None, :],
        -jnp.inf,
    )
    carried_logs = forget_sums + prior_peak[..., None]
    row_peak = jnp.maximum(carried_logs, jnp.max(pair_logs, axis=-1))
    inner_weights = jnp.exp(pair_logs - row_peak[..., None])
    carried_weights = jnp.exp(carried_logs - row_peak)
    scores = inner_weights * jnp.einsum(
        "bcld,bcsd->bcls", query_blocks, key_blocks, precision=HIGHEST_PRECISION
    )
    numerator = carried_weights[..., None] * jnp.einsum(
        "bcvk,bclk->bclv", prior_state, query_blocks, precision=HIGHEST_PRECISION
    ) + jnp.einsum("bcls,bcsv->bclv", scores, value_blocks, precision=HIGHEST_PRECISION)
    return numerator.reshape(members, tokens, head_width)


def shards(
    activations,
    norm_gain,
    w_conv_gate,
    w_conv_mult,
    w_conv_in,
    conv_taps,
    w_query,
    w_key,
    w_value,
    w_input_gate,
    w_forget_gate,
    gate_bias,
    decay_shift,
    head_gain,
    w_out_conv,
    w_out_mem,
):
    group_index = lax.axis_index(("fs", "tp"))
    heads_here = MEMORY_HEADS // (lax.axis_size("fs") * lax.axis_size("tp"))
    channels = w_conv_gate.shape[1]
    sequences = lax.all_gather(activations, "fs", axis=0, tiled=True)
    seq_count = sequences.shape[0]
    tokens = sequences.shape[1]
    model_width = sequences.shape[2]
    row_count = seq_count * tokens
    flat_rows = sequences.reshape(row_count, model_width).astype(jnp.float32)
    normed = (
        flat_rows
        * lax.rsqrt(jnp.mean(flat_rows * flat_rows, axis=-1, keepdims=True) + EPSILON)
        * norm_gain
    ).astype(jnp.bfloat16)
    pieces = (
        lax.all_gather(w_conv_gate, "sp", axis=0, tiled=True),
        lax.all_gather(w_conv_mult, "sp", axis=0, tiled=True),
        lax.all_gather(w_conv_in, "sp", axis=0, tiled=True),
        lax.all_gather(w_query, "sp", axis=0, tiled=True),
        lax.all_gather(w_key, "sp", axis=0, tiled=True),
        lax.all_gather(w_value, "sp", axis=0, tiled=True),
    )
    projected = tuple(
        (jnp.dot(normed, shard_piece, preferred_element_type=jnp.float32) for shard_piece in pieces)
    )
    conv_gate, conv_mult, conv_in, query, keys_proj, value = [
        tensor.astype(jnp.bfloat16).reshape(seq_count, tokens, -1) for tensor in projected
    ]
    product = (conv_mult.astype(jnp.float32) * conv_in.astype(jnp.float32)).astype(jnp.bfloat16)
    ntaps = conv_taps.shape[0]
    rim_rows = from_behind(product[:, tokens - (ntaps - 1) :, :], "sp", 1)
    padded = jnp.concatenate([rim_rows, product], axis=1).astype(jnp.float32)
    tap_weights = lax.dynamic_slice_in_dim(conv_taps, group_index * channels, channels, 1)
    mixed_sum = jnp.zeros((seq_count, tokens, channels), jnp.float32)
    for tap_index in range(ntaps):
        mixed_sum = (
            mixed_sum + tap_weights[tap_index] * padded[:, tap_index : tap_index + tokens, :]
        )
    conv_out = (conv_gate.astype(jnp.float32) * mixed_sum).astype(jnp.bfloat16)
    entry_cols = lax.dynamic_slice_in_dim(w_input_gate, group_index * heads_here, heads_here, 1)
    forget_cols = lax.dynamic_slice_in_dim(w_forget_gate, group_index * heads_here, heads_here, 1)
    gate_values = jnp.dot(
        normed,
        jnp.concatenate([entry_cols, forget_cols], axis=1),
        preferred_element_type=jnp.float32,
    ).reshape(seq_count, tokens, 2 * heads_here)
    bias_rows = lax.dynamic_slice_in_dim(gate_bias, group_index * heads_here, heads_here, 1)
    decay_rows = lax.dynamic_slice_in_dim(decay_shift, group_index * heads_here, heads_here, 2)
    entry = gate_values[..., :heads_here] + bias_rows[0]
    log_forget = jax.nn.log_sigmoid(gate_values[..., heads_here:] + bias_rows[1]) + decay_rows
    cell = memory_cell(
        head_rows(query, seq_count, heads_here),
        head_rows(keys_proj, seq_count, heads_here),
        head_rows(value, seq_count, heads_here),
        gate_rows(entry, seq_count, heads_here),
        gate_rows(log_forget, seq_count, heads_here),
    )
    cell = cell * lax.rsqrt(jnp.mean(cell * cell, axis=-1, keepdims=True) + EPSILON)
    gain_rows = lax.dynamic_slice_in_dim(
        head_gain, group_index * heads_here * HEAD_DIM, heads_here * HEAD_DIM, 0
    ).reshape(1, heads_here, 1, HEAD_DIM)
    scaled = cell.reshape(seq_count, heads_here, tokens, HEAD_DIM) * gain_rows
    mem_out = (
        scaled.transpose(0, 2, 1, 3)
        .reshape(seq_count, tokens, heads_here * HEAD_DIM)
        .astype(jnp.bfloat16)
    )
    conv_seq, mem_seq = (
        lax.all_to_all(conv_out, "fs", split_axis=0, concat_axis=2, tiled=True),
        lax.all_to_all(mem_out, "fs", split_axis=0, concat_axis=2, tiled=True),
    )
    rows_conv, rows_mem = (
        lax.all_gather(w_out_conv, "fs", axis=0, tiled=True),
        lax.all_gather(w_out_mem, "fs", axis=0, tiled=True),
    )
    full_conv, full_mem = (
        lax.all_gather(rows_conv, "sp", axis=1, tiled=True),
        lax.all_gather(rows_mem, "sp", axis=1, tiled=True),
    )
    conv_flat = conv_seq[0]
    mem_flat = mem_seq[0]
    output = lax.psum_scatter(
        (
            jnp.dot(conv_flat, full_conv, preferred_element_type=jnp.float32)
            + jnp.dot(mem_flat, full_mem, preferred_element_type=jnp.float32)
        ).astype(jnp.bfloat16),
        "tp",
        scatter_dimension=0,
        tiled=True,
    ).astype(jnp.float32)
    return output.astype(jnp.bfloat16).reshape(1, output.shape[0], -1)


def solution(mesh):
    return jax.shard_map(
        shards,
        mesh=mesh,
        in_specs=(
            P("fs", "sp", None),
            P(),
            P("sp", ("fs", "tp")),
            P("sp", ("fs", "tp")),
            P("sp", ("fs", "tp")),
            P(),
            P("sp", ("fs", "tp")),
            P("sp", ("fs", "tp")),
            P("sp", ("fs", "tp")),
            P(),
            P(),
            P(),
            P(None, "sp", None),
            P(),
            P(("fs", "tp"), "sp"),
            P(("fs", "tp"), "sp"),
        ),
        out_specs=P("fs", ("sp", "tp"), None),
        check_vma=False,
    )
```

profile of v0, /device:TPU:1, one launch (start us, length us, event | category | flops | bytes accessed | tf_op | source)
XLA Modules:
  0.0 249.6 jit_solution(10992935933422332303)
XLA Ops:
  6.5 0.7 all-gather.8.cloned.1.call-update
  7.4 0.8 constant_dynamic-slice_fusion.4
  8.1 0.6 fusion.51
  8.7 15.5 %all_gather.58 = bf16[2048,128]{1,0:T(8,128)(2,1)S(1)} all-gather(bf16[512,128]{1,0:T(8,128)(2,1)} %param.27), channel_id=1, replica_groups=mesh['sp'=4,'fs'=4,'tp'=2] {'sp'}, dimensions={0}, use_global_device_ids=true | all-gather | bytes 655360 | tf_op jit(solution)/shard_map/all_gather | solution.py:162
  24.3 12.1 %all_gather.57 = bf16[2048,128]{1,0:T(8,128)(2,1)S(1)} all-gather(bf16[512,128]{1,0:T(8,128)(2,1)} %param.28), channel_id=1, replica_groups=mesh['sp'=4,'fs'=4,'tp'=2] {'sp'}, dimensions={0}, use_global_device_ids=true | all-gather | bytes 655360 | tf_op jit(solution)/shard_map/all_gather | solution.py:163
  36.3 0.8 constant_dynamic-slice_fusion.5
  37.1 26.5 %all-gather.8.cloned.1.call-done = bf16[4,256,2048]{2,1,0:T(8,128)(2,1)} async-done(((bf16[1,256,2048]{2,1,0:T(8,128)(2,1)}), bf16[4,256,2048]{2,1,0:T(8,128)(2,1)}) %all-gather.8.cloned.1.call-update) | async-done | bytes 4194320 | tf_op jit(solution)/shard_map/all_gather | solution.py:146
  63.7 3.2 %multiply_reduce_fusion = f32[4,256]{1,0:T(4,128)S(1)} fusion(bf16[4,256,2048]{2,1,0:T(8,128)(2,1)} %all-gather.8.cloned.1.call-done), kind=kLoop, calls=%fused_computation.34 | loop fusion | flops 6290432 | bytes 4198400 | tf_op jit(solution)/shard_map/reduce_sum | solution.py:154
  66.9 0.2 copy-done.4
  67.1 1.3 fusion.15
  68.4 2.2 fusion.43
  70.6 0.9 reduce_window_sum.11
  71.6 0.2 slice_reduce_fusion
  71.8 0.2 fusion.46
  72.1 3.2 %fusion.14 = bf16[1024,2048]{1,0:T(8,128)(2,1)S(1)} fusion(bf16[4,256,2048]{2,1,0:T(8,128)(2,1)} %all-gather.8.cloned.1.call-done, f32[2048]{0:T(1024)S(1)} %copy-done.8, f32[1024]{0:T(1024)S(1)} %bitcast.163), kind=kLoop, calls=%fused_computation.32 | loop fusion | flops 8388608 | bytes 8400896 | tf_op jit(solution)/shard_map/convert_element_type | solution.py:156
  75.3 1.3 fusion.22
  76.6 1.2 convolution_convert_fusion.2
  77.8 0.1 copy.35
  78.0 2.0 convolution_bitcast_fusion
  80.0 1.1 while.39
  80.1 0.1 fusion.80
  80.4 0.1 fusion.80
  80.6 0.1 fusion.80
  80.9 0.1 fusion.80
  81.1 0.7 copy-done.3
  81.9 8.6 %all_gather.55 = bf16[512,512]{1,0:T(8,128)(2,1)} all-gather(bf16[128,512]{1,0:T(8,128)(2,1)S(1)} %copy-done.6), channel_id=1, replica_groups=mesh['sp'=4,'fs'=4,'tp'=2] {'fs'}, dimensions={0}, use_global_device_ids=true | all-gather | bytes 655360 | tf_op jit(solution)/shard_map/all_gather | solution.py:215
  90.6 9.3 %all_gather.66 = bf16[512,512]{1,0:T(8,128)(2,1)} all-gather(bf16[128,512]{1,0:T(8,128)(2,1)S(1)} %copy-done.7), channel_id=1, replica_groups=mesh['sp'=4,'fs'=4,'tp'=2] {'fs'}, dimensions={0}, use_global_device_ids=true | all-gather | bytes 655360 | tf_op jit(solution)/shard_map/all_gather | solution.py:216
  100.0 17.7 %all_gather.65 = bf16[2048,128]{1,0:T(8,128)(2,1)} all-gather(bf16[512,128]{1,0:T(8,128)(2,1)} %param.26), channel_id=1, replica_groups=mesh['sp'=4,'fs'=4,'tp'=2] {'sp'}, dimensions={0}, use_global_device_ids=true | all-gather | bytes 655360 | tf_op jit(solution)/shard_map/all_gather | solution.py:161
  117.7 16.9 %all_gather.53 = bf16[2048,128]{1,0:T(8,128)(2,1)S(1)} all-gather(bf16[512,128]{1,0:T(8,128)(2,1)} %param.23), channel_id=1, replica_groups=mesh['sp'=4,'fs'=4,'tp'=2] {'sp'}, dimensions={0}, use_global_device_ids=true | all-gather | bytes 655360 | tf_op jit(solution)/shard_map/all_gather | solution.py:159
  134.6 20.7 %all_gather.54 = bf16[2048,128]{1,0:T(8,128)(2,1)S(1)} all-gather(bf16[512,128]{1,0:T(8,128)(2,1)} %param.24), channel_id=1, replica_groups=mesh['sp'=4,'fs'=4,'tp'=2] {'sp'}, dimensions={0}, use_global_device_ids=true | all-gather | bytes 655360 | tf_op jit(solution)/shard_map/all_gather | solution.py:160
  155.4 0.9 dynamic_slice.55
  156.3 20.6 %all_gather.52 = bf16[2048,128]{1,0:T(8,128)(2,1)} all-gather(bf16[512,128]{1,0:T(8,128)(2,1)} %param.22), channel_id=1, replica_groups=mesh['sp'=4,'fs'=4,'tp'=2] {'sp'}, dimensions={0}, use_global_device_ids=true | all-gather | bytes 655360 | tf_op jit(solution)/shard_map/all_gather | solution.py:158
  176.9 0.6 dynamic-slice
  178.1 4.2 %convolution_convert_fusion = bf16[1024,128]{1,0:T(8,128)(2,1)} fusion(bf16[1024,2048]{1,0:T(8,128)(2,1)} %copy-done.1, bf16[2048,128]{1,0:T(8,128)(2,1)} %all_gather.65), kind=kOutput, calls=%fused_computation.45 | convolution fusion | flops 537001984 | bytes 4980736 | tf_op jit(solution)/shard_map/dot_general | solution.py:166
  182.4 1.2 fusion.26
  183.6 1.3 fusion.25
  184.9 0.1 copy.31
  185.0 0.1 slice.48
  185.1 3.1 %collective-permute-start = (bf16[4,2,128]{1,2,0:T(8,128)(2,1)S(1)}, bf16[4,2,128]{1,2,0:T(8,128)(2,1)S(1)}, u32[]{:S(2)}, u32[]{:S(2)}) collective-permute-start(bf16[4,2,128]{1,2,0:T(8,128)(2,1)S(1)} %slice.48), channel_id=1, source_target_pairs={{0,8},{8,16},{16,24},{1,9},{9,17},{17,25},{2,10},{10,18},{18,26},{... | collective-permute-start | bytes 6152 | tf_op jit(solution)/shard_map/ppermute | solution.py:33
  188.2 3.7 %convolution_convert_fusion.5 = bf16[1024,128]{1,0:T(8,128)(2,1)S(1)} fusion(bf16[1024,2048]{1,0:T(8,128)(2,1)} %copy-done.1, bf16[2048,128]{1,0:T(8,128)(2,1)} %all_gather.52), kind=kOutput, calls=%fused_computation.56 | convolution fusion | flops 537001984 | bytes 4980736 | tf_op jit(solution)/shard_map/dot_general | solution.py:166
  191.9 0.4 fusion.33
  192.3 0.2 dynamic-update-slice
  192.6 0.2 dynamic-update-slice.1
  192.8 7.5 %all-reduce.2 = (f32[16]{0:T(128)S(1)}, f32[16]{0:T(128)S(1)}) all-reduce(f32[16]{0:T(128)S(1)} %dynamic-update-slice, f32[16]{0:T(128)S(1)} %dynamic-update-slice.1), channel_id=2, replica_groups=mesh['sp'=4,'fs'=4,'tp'=2] {'sp'}, use_global_device_ids=true, to_apply=%add | all-reduce | flops 32 | bytes 256
  200.4 0.1 copy.33
  200.6 0.2 maximum_convert_fusion
  200.8 1.1 fusion.31
  201.9 3.4 %all-to-all-start = ((bf16[4,256,128]{1,2,0:T(8,128)(2,1)}), bf16[4,256,128]{1,2,0:T(8,128)(2,1)S(1)}, u32[]{:S(2)}, u32[]{:S(2)}) async-start(bf16[4,256,128]{1,2,0:T(8,128)(2,1)} %fusion.31), calls=%async_computation | async-start | bytes 524288 | tf_op jit(solution)/shard_map/all_to_all | solution.py:211
  205.3 3.4 %while.40 = (s32[]{:T(128)}, f32[4]{0:T(128)S(1)}, f32[4]{0:T(128)S(1)}, f32[4,128,128]{2,1,0:T(8,128)S(1)}, s32[]{:T(128)}, /*index=5*/f32[4,4]{1,0:T(4,128)S(1...) while((s32[]{:T(128)}, f32[4]{0:T(128)S(1)}, f32[4]{0:T(128)S(1)}, ...), condition=%wide.region_6.7_spmd.clone, body=%wide.region_5.6_spmd.clone.sunk | while | flops 327728 | bytes 786793 | solution.py:27
  205.4 1.1 fusion.81
  206.5 1.1 fusion.81
  207.7 1.1 fusion.81
  208.8 0.1 copy.37
  209.0 0.1 multiply_add_fusion
  209.1 0.6 convolution_multiply_fusion.1
  209.6 0.4 fusion.53
  210.0 1.3 multiply_reduce_fusion.1
  211.3 0.2 copy.39
  211.6 0.8 multiply_convert_fusion.2
  212.4 3.5 %all-to-all-start.1 = ((bf16[4,256,128]{1,2,0:T(8,128)(2,1)}), bf16[4,256,128]{1,2,0:T(8,128)(2,1)S(1)}, u32[]{:S(2)}, u32[]{:S(2)}) async-start(bf16[4,256,128]{1,2,0:T(8,128)(2,1)} %multiply_convert_fusion.2), calls=%async_computation.1 | async-start | bytes 524288 | tf_op jit(solution)/shard_map/all_to_all | solution.py:212
  216.0 2.3 fusion.52
  218.3 10.6 %all-gather.12.cloned.1.call-done = bf16[512,2048]{1,0:T(8,128)(2,1)} async-done(((bf16[512,512]{1,0:T(8,128)(2,1)}), bf16[512,2048]{1,0:T(8,128)(2,1)}) %all-gather.12.cloned.1.call-update) | async-done | bytes 2097168 | tf_op jit(solution)/shard_map/all_gather | solution.py:220
  228.9 3.3 %fusion.19 = bf16[256,2048]{1,0:T(8,128)(2,1)} fusion(f32[256,2048]{1,0:T(8,128)S(1)} %fusion.52, bf16[256,512]{0,1:T(8,128)(2,1)S(1)} %bitcast.159, bf16[512,2048]{1,0:T(8,128)(2,1)} %all-gather.12.cloned.1.call-done), kind=kOutput, calls=%fused_computation.40 | convolution fusion | flops 537919488 | bytes 5505024 | tf_op jit(solution)/shard_map/dot_general | solution.py:227
  232.2 10.8 %reduce-scatter.2.cloned.1.call-done = bf16[128,2048]{1,0:T(8,128)(2,1)} async-done(((bf16[256,2048]{1,0:T(8,128)(2,1)}), bf16[128,2048]{1,0:T(8,128)(2,1)}) %reduce-scatter.2.cloned.1.call-update) | async-done | bytes 524304 | tf_op jit(solution)/shard_map/reduce_scatter | solution.py:224
  (87 shorter events, 1.7 us)
Async XLA Ops:
  6.5 149.8 %copy-start = (f32[3,1024]{1,0:T(4,128)S(1)}, f32[3,1024]{1,0:T(4,128)}, u32[]{:S(2)}) copy-start(f32[3,1024]{1,0:T(4,128)} %param.25) | copy-start | bytes 36868
  6.5 60.4 %copy-start.8 = (f32[2048]{0:T(1024)S(1)}, f32[2048]{0:T(1024)}, u32[]{:S(2)}) copy-start(f32[2048]{0:T(1024)} %param.21) | copy-start | bytes 24580
  6.5 57.1 %all-gather.8.cloned.1.call-start = ((), (), s32[]{:S(2)}) async-start(), calls=%async_computation.3 | async-start | bytes 5242880 | tf_op jit(solution)/shard_map/all_gather | solution.py:146
  7.3 198.0 %all-gather.14.cloned.1.call-start = ((), (), s32[]{:S(2)}) async-start(), calls=%async_computation.7 | async-start | bytes 1310720 | tf_op jit(solution)/shard_map/all_gather | solution.py:18
  63.7 3.4 %copy-start.4 = (bf16[4,256,2048]{2,1,0:T(8,128)(2,1)S(1)}, bf16[4,256,2048]{2,1,0:T(8,128)(2,1)}, u32[]{:S(2)}) copy-start(bf16[4,256,2048]{2,1,0:T(8,128)(2,1)} %all-gather.8.cloned.1.call-done) | copy-start | bytes 12582916
  75.3 2.5 %copy-start.1 = (bf16[1024,2048]{1,0:T(8,128)(2,1)}, bf16[1024,2048]{1,0:T(8,128)(2,1)S(1)}, u32[]{:S(2)}) copy-start(bf16[1024,2048]{1,0:T(8,128)(2,1)S(1)} %fusion.14) | copy-start | bytes 12582916
  78.0 3.8 %copy-start.6 = (bf16[128,512]{1,0:T(8,128)(2,1)S(1)}, bf16[128,512]{1,0:T(8,128)(2,1)}, u32[]{:S(2)}) copy-start(bf16[128,512]{1,0:T(8,128)(2,1)} %param.34) | copy-start | bytes 393220
  80.0 10.5 %copy-start.7 = (bf16[128,512]{1,0:T(8,128)(2,1)S(1)}, bf16[128,512]{1,0:T(8,128)(2,1)}, u32[]{:S(2)}) copy-start(bf16[128,512]{1,0:T(8,128)(2,1)} %param.35) | copy-start | bytes 393220
  81.1 0.7 copy-start.3
  81.1 95.8 %copy-start.9 = (u32[32]{0:T(128)S(1)}, u32[32]{0:T(128)}, u32[]{:S(2)}) copy-start(u32[32]{0:T(128)} %constant.88) | copy-start | bytes 388
  81.8 134.2 %all-gather.10.cloned.1.call-start = ((), (), s32[]{:S(2)}) async-start(), calls=%async_computation.4 | async-start | bytes 2621440 | tf_op jit(solution)/shard_map/all_gather | solution.py:219
  90.5 138.4 %all-gather.12.cloned.1.call-start = ((), (), s32[]{:S(2)}) async-start(), calls=%async_computation.5 | async-start | bytes 2621440 | tf_op jit(solution)/shard_map/all_gather | solution.py:220
  155.4 27.0 %copy-start.2 = (bf16[1024,2048]{1,0:T(8,128)(2,1)S(1)}, bf16[1024,2048]{1,0:T(8,128)(2,1)}, u32[]{:S(2)}) copy-start(bf16[1024,2048]{1,0:T(8,128)(2,1)} %copy-done.1) | copy-start | bytes 12582916
  185.1 15.4 %collective-permute-start = (bf16[4,2,128]{1,2,0:T(8,128)(2,1)S(1)}, bf16[4,2,128]{1,2,0:T(8,128)(2,1)S(1)}, u32[]{:S(2)}, u32[]{:S(2)}) collective-permute-start(bf16[4,2,128]{1,2,0:T(8,128)(2,1)S(1)} %slice.48), channel_id=1, source_target_pairs={{0,8},{8,16},{16,24},{1,9},{9,17},{17,25},{2,10},{10,18},{18,26},{... | collective-permute-start | bytes 6152 | tf_op jit(solution)/shard_map/ppermute | solution.py:33
  200.5 8.5 %copy-start.5 = (bf16[1024,128]{1,0:T(8,128)(2,1)S(1)}, bf16[1024,128]{1,0:T(8,128)(2,1)}, u32[]{:S(2)}) copy-start(bf16[1024,128]{1,0:T(8,128)(2,1)} %convolution_convert_fusion) | copy-start | bytes 786436
  201.9 10.6 %all-to-all-start = ((bf16[4,256,128]{1,2,0:T(8,128)(2,1)}), bf16[4,256,128]{1,2,0:T(8,128)(2,1)S(1)}, u32[]{:S(2)}, u32[]{:S(2)}) async-start(bf16[4,256,128]{1,2,0:T(8,128)(2,1)} %fusion.31), calls=%async_computation | async-start | bytes 524288 | tf_op jit(solution)/shard_map/all_to_all | solution.py:211
  212.4 16.4 %all-to-all-start.1 = ((bf16[4,256,128]{1,2,0:T(8,128)(2,1)}), bf16[4,256,128]{1,2,0:T(8,128)(2,1)S(1)}, u32[]{:S(2)}, u32[]{:S(2)}) async-start(bf16[4,256,128]{1,2,0:T(8,128)(2,1)} %multiply_convert_fusion.2), calls=%async_computation.1 | async-start | bytes 524288 | tf_op jit(solution)/shard_map/all_to_all | solution.py:212
  216.0 27.1 %reduce-scatter.2.cloned.1.call-start = ((), (), s32[]{:S(2)}) async-start(), calls=%async_computation.6 | async-start | bytes 1572864 | tf_op jit(solution)/shard_map/reduce_scatter | solution.py:224
Sparse Core Ops, SparseCore 0:
  9.2 54.4 all-gather.7
  81.9 29.9 all-gather.13
  113.5 69.1 all-gather.9
  184.1 44.6 all-gather.11
  232.3 10.6 reduce-scatter.1
where the time goes:
time: 251 us; the launch traced here: 250 us
  blocking collectives  129 us (51%)
  waiting for transfers between devices  48.8 us (19%)
  matrix products  24 us (10%)
  other arithmetic  16.5 us (7%)
  between operations  14.2 us (6%)
  starting transfers between devices  10.1 us (4%)
  local copies, waits for them, and re-layouts  6.76 us (3%)
    all_gather x1, waiting for transfers between devices, shards(): sequences = lax.all_gather(activations, 'fs', axis=0, tiled=True)  26.5 us
    all_gather x1, blocking collectives, shards(): lax.all_gather(w_conv_in, 'sp', axis=0, tiled=True)  20.7 us
    all_gather x1, blocking collectives, shards(): lax.all_gather(w_conv_gate, 'sp', axis=0, tiled=True)  20.6 us
    all_gather x1, blocking collectives, shards(): lax.all_gather(w_query, 'sp', axis=0, tiled=True)  17.7 us
    all_gather x1, blocking collectives, shards(): lax.all_gather(w_conv_mult, 'sp', axis=0, tiled=True)  16.9 us
    all_gather x1, blocking collectives, shards(): lax.all_gather(w_key, 'sp', axis=0, tiled=True)  15.5 us
    dot_general x6, matrix products, shards(): jnp.dot(normed, shard_piece, preferred_element_type=jnp.float32)  12.9 us
    all_gather x1, blocking collectives, shards(): lax.all_gather(w_value, 'sp', axis=0, tiled=True)  12.1 us
  transfers between devices with their start and end apart: 8, of which 3 were waited for; matrix products, arithmetic and copies ran while one was open for 10% of the time, Pallas kernels for 0%

commit v1 on v0

--- a/solution.py
+++ b/solution.py
@@ -1,6 +1,10 @@
+import functools
+
 import jax
 import jax.numpy as jnp
 from jax import lax
+from jax.experimental import pallas as pl
+from jax.experimental.pallas import tpu as pltpu
 from jax.sharding import PartitionSpec as P
 
 MEMORY_HEADS = 8
@@ -120,6 +124,437 @@
         "bcvk,bclk->bclv", prior_state, query_blocks, precision=HIGHEST_PRECISION
     ) + jnp.einsum("bcls,bcsv->bclv", scores, value_blocks, precision=HIGHEST_PRECISION)
     return numerator.reshape(members, tokens, head_width)
+
+
+MESH = pl.DeviceIdType.MESH
+
+
+def greet(peers):
+    barrier = pltpu.get_barrier_semaphore()
+    total = 0
+    for there, peer in peers:
+        if there is None:
+            pl.semaphore_signal(barrier, inc=1, device_id=peer, device_id_type=MESH)
+            total = total + 1
+        else:
+
+            @pl.when(there)
+            def _(peer=peer):
+                pl.semaphore_signal(barrier, inc=1, device_id=peer, device_id_type=MESH)
+
+            total = total + there.astype(jnp.int32)
+    pl.semaphore_wait(barrier, total)
+
+
+def gather_kernel(
+    ns,
+    nf,
+    cuts,
+    act_ref,
+    gain_ref,
+    w0_ref,
+    w1_ref,
+    w2_ref,
+    w3_ref,
+    w4_ref,
+    w5_ref,
+    wg_ref,
+    wc_ref,
+    wm_ref,
+    proj_ref,
+    gate_ref,
+    wo_ref,
+    acts,
+    normed,
+    wbuf,
+    total,
+    local_sem,
+    a_send,
+    a_recv,
+    ad_send,
+    ad_recv,
+    w_send,
+    w_recv,
+    o_send,
+    o_recv,
+    p_send,
+    p_recv,
+    d_send,
+    d_recv,
+):
+    sp, fs, tp = (lax.axis_index("sp"), lax.axis_index("fs"), lax.axis_index("tp"))
+    g = fs * 2 + tp
+    depth, cols = w0_ref.shape
+    width = 6 * cols
+    cut = width // cuts
+    tokens, model = act_ref.shape
+    half = tokens // 2
+    ocols = wc_ref.shape[1]
+    partner = (sp, fs, 1 - tp)
+    has_up, has_down = (sp + 1 < ns, sp > 0)
+    up, down = ((sp + 1, fs, tp), (sp - 1, fs, tp))
+
+    own_rows = pl.ds(pl.multiple_of(sp * depth, depth), depth)
+    locals_ = []
+    for j, ref in enumerate((w0_ref, w1_ref, w2_ref, w3_ref, w4_ref, w5_ref)):
+        locals_.append(
+            pltpu.make_async_copy(
+                ref, wbuf.at[own_rows, pl.ds(j * cols, cols)], local_sem.at[j]
+            )
+        )
+    own_ocols = pl.ds(pl.multiple_of(sp * ocols, ocols), ocols)
+    for m, ref in enumerate((wc_ref, wm_ref)):
+        locals_.append(
+            pltpu.make_async_copy(ref, wo_ref.at[g, m, :, own_ocols], local_sem.at[6 + m])
+        )
+    locals_.append(pltpu.make_async_copy(act_ref, acts.at[fs], local_sem.at[8]))
+    for copy in locals_:
+        copy.start()
+
+    fs_peers = [(None, (sp, lax.rem(fs + off, nf), tp)) for off in range(1, nf)]
+    greet(fs_peers + [(None, partner), (has_up, up), (has_down, down)])
+
+    my_half = pl.ds(pl.multiple_of(tp * half, half), half)
+    other_half = pl.ds(pl.multiple_of((1 - tp) * half, half), half)
+
+    def act_copy(off, src_f):
+        return pltpu.make_async_remote_copy(
+            act_ref.at[my_half],
+            acts.at[src_f, my_half],
+            a_send.at[off - 1],
+            a_recv.at[off - 1],
+            device_id=(sp, lax.rem(fs + off, nf), tp),
+            device_id_type=MESH,
+        )
+
+    def act_relay(off, src_f, rows):
+        return pltpu.make_async_remote_copy(
+            acts.at[src_f, rows],
+            acts.at[src_f, rows],
+            ad_send.at[off - 1],
+            ad_recv.at[off - 1],
+            device_id=partner,
+            device_id_type=MESH,
+        )
+
+    def w_copy(side, d, owner, k):
+        rows = pl.ds(pl.multiple_of(owner * depth, depth), depth)
+        place = wbuf.at[rows, pl.ds(k * cut, cut)]
+        return pltpu.make_async_remote_copy(
+            place,
+            place,
+            w_send.at[side, d, k],
+            w_recv.at[side, d, k],
+            device_id=(up, down)[side],
+            device_id_type=MESH,
+        )
+
+    def o_copy(side, d, owner):
+        place = wo_ref.at[g, :, :, pl.ds(pl.multiple_of(owner * ocols, ocols), ocols)]
+        return pltpu.make_async_remote_copy(
+            place,
+            place,
+            o_send.at[side, d],
+            o_recv.at[side, d],
+            device_id=(up, down)[side],
+            device_id_type=MESH,
+        )
+
+    def p_copy(owner, off, src_g):
+        place = wo_ref.at[src_g, :, :, pl.ds(pl.multiple_of(owner * ocols, ocols), ocols)]
+        return pltpu.make_async_remote_copy(
+            place,
+            place,
+            p_send.at[owner, off - 1],
+            p_recv.at[owner, off - 1],
+            device_id=(sp, lax.rem(fs + off, nf), tp),
+            device_id_type=MESH,
+        )
+
+    def d_copy(owner, off, src_g):
+        place = wo_ref.at[src_g, :, :, pl.ds(pl.multiple_of(owner * ocols, ocols), ocols)]
+        return pltpu.make_async_remote_copy(
+            place,
+            place,
+            d_send.at[owner, off],
+            d_recv.at[owner, off],
+            device_id=partner,
+            device_id_type=MESH,
+        )
+
+    def origin(off):
+        return lax.rem(fs + nf - off, nf)
+
+    def sends(side, d):
+        if side == 0:
+            return (sp - d >= 0) & has_up
+        return (sp + d < ns) & has_down
+
+    def owner_of(side, d):
+        return sp - d if side == 0 else sp + d
+
+    def arrives(side, d):
+        return (sp - d >= 0) if side == 0 else (sp + d < ns)
+
+    for off in range(1, nf):
+        act_copy(off, fs).start()
+    for copy in locals_:
+        copy.wait()
+
+    def send_z(side, d):
+        @pl.when(sends(side, d))
+        def _():
+            o_copy(side, d, owner_of(side, d)).start()
+
+    def send_w(side, d, k):
+        @pl.when(sends(side, d))
+        def _():
+            w_copy(side, d, owner_of(side, d), k).start()
+
+    for side in range(2):
+        send_z(side, 0)
+    for k in range(cuts):
+        for side in range(2):
+            send_w(side, 0, k)
+
+    def spread(owner):
+        for off in range(1, nf):
+            p_copy(owner, off, g).start()
+        d_copy(owner, 0, g).start()
+
+    spread(sp)
+    for off in range(1, nf):
+        act_copy(off, origin(off)).wait_recv()
+        act_relay(off, origin(off), my_half).start()
+
+    def z_round(d):
+        for side in range(2):
+
+            @pl.when(arrives(side, d))
+            def _():
+                owner = owner_of(side, d)
+                o_copy(side, d - 1, owner).wait_recv()
+                if d < ns - 1:
+                    send_z(side, d)
+                spread(owner)
+
+    for off in range(1, nf):
+        act_relay(off, origin(off), other_half).wait_recv()
+
+    step = 64
+
+    def norm_rows(i, carry):
+        f = i // (tokens // step)
+        rows = pl.ds(pl.multiple_of(lax.rem(i, tokens // step) * step, step), step)
+        x = acts[f, rows, :].astype(jnp.float32)
+        scale = lax.rsqrt(jnp.mean(x * x, axis=-1, keepdims=True) + EPSILON)
+        out = (x * scale * gain_ref[...]).astype(jnp.bfloat16)
+        normed[pl.ds(pl.multiple_of(i * step, step), step), :] = out
+        return carry
+
+    lax.fori_loop(0, nf * tokens // step, norm_rows, 0)
+    tile = tokens
+
+    def multiply(owner, first):
+        rows = pl.ds(pl.multiple_of(owner * depth, depth), depth)
+
+        def body(i, carry):
+            here = pl.ds(pl.multiple_of(i * tile, tile), tile)
+            part = jnp.dot(
+                normed[here, rows], wbuf[rows, :], preferred_element_type=jnp.float32
+            )
+            total[here, :] = part if first else total[here, :] + part
+            return carry
+
+        lax.fori_loop(0, nf, body, 0)
+
+    z_round(1)
+    multiply(sp, True)
+
+    def gates(i, carry):
+        here = pl.ds(pl.multiple_of(i * tile, tile), tile)
+        gate_ref[here, :] = jnp.dot(
+            normed[here, :], wg_ref[...], preferred_element_type=jnp.float32
+        )
+        return carry
+
+    lax.fori_loop(0, nf, gates, 0)
+
+    for d in range(1, ns):
+        for k in range(cuts):
+            for side in range(2):
+
+                @pl.when(arrives(side, d))
+                def _():
+                    w_copy(side, d - 1, owner_of(side, d), k).wait_recv()
+                    if d < ns - 1:
+                        send_w(side, d, k)
+
+        for side in range(2):
+
+            @pl.when(arrives(side, d))
+            def _():
+                multiply(owner_of(side, d), False)
+
+        if d + 1 < ns:
+            z_round(d + 1)
+
+    def round_rows(i, carry):
+        here = pl.ds(pl.multiple_of(i * tile, tile), tile)
+        proj_ref[here, :] = total[here, :].astype(jnp.bfloat16)
+        return carry
+
+    lax.fori_loop(0, nf, round_rows, 0)
+
+    def collect(s, carry):
+        for off in range(1, nf):
+            src_g = origin(off) * 2 + tp
+            p_copy(s, off, src_g).wait_recv()
+            d_copy(s, off, src_g).start()
+        return carry
+
+    lax.fori_loop(0, ns, collect, 0)
+
+    def finish(s, carry):
+        for off in range(nf):
+            d_copy(s, off, origin(off) * 2 + 1 - tp).wait_recv()
+            d_copy(s, off, origin(off) * 2 + tp).wait_send()
+        for off in range(1, nf):
+            p_copy(s, off, g).wait_send()
+        return carry
+
+    lax.fori_loop(0, ns, finish, 0)
+    for off in range(1, nf):
+        act_copy(off, fs).wait_send()
+        act_relay(off, origin(off), my_half).wait_send()
+    for side in range(2):
+        for d in range(ns - 1):
+
+            @pl.when(sends(side, d))
+            def _():
+                o_copy(side, d, owner_of(side, d)).wait_send()
+                for k in range(cuts):
+                    w_copy(side, d, owner_of(side, d), k).wait_send()
+
+
+def gather_and_project(act, gain, weights, gate_weights, w_out_conv, w_out_mem):
+    ns, nf = (lax.axis_size("sp"), lax.axis_size("fs"))
+    tokens, model = act.shape
+    depth, cols = weights[0].shape
+    rows, ocols = w_out_conv.shape
+    count = nf * tokens
+    cuts = 2
+    vmem = pl.BlockSpec(memory_space=pltpu.VMEM)
+    dma = pltpu.SemaphoreType.DMA
+    return pl.pallas_call(
+        functools.partial(gather_kernel, ns, nf, cuts),
+        out_shape=(
+            jax.ShapeDtypeStruct((count, 6 * cols), jnp.bfloat16),
+            jax.ShapeDtypeStruct((count, gate_weights.shape[1]), jnp.float32),
+            jax.ShapeDtypeStruct((nf * 2, 2, rows, ns * ocols), jnp.bfloat16),
+        ),
+        in_specs=[vmem] * 11,
+        out_specs=(vmem, vmem, pl.BlockSpec(memory_space=pl.ANY)),
+        scratch_shapes=[
+            pltpu.VMEM((nf, tokens, model), jnp.bfloat16),
+            pltpu.VMEM((count, model), jnp.bfloat16),
+            pltpu.VMEM((ns * depth, 6 * cols), jnp.bfloat16),
+            pltpu.VMEM((count, 6 * cols), jnp.float32),
+            dma((9,)),
+            dma((nf - 1,)),
+            dma((nf - 1,)),
+            dma((nf - 1,)),
+            dma((nf - 1,)),
+            dma((2, ns - 1, cuts)),
+            dma((2, ns - 1, cuts)),
+            dma((2, ns - 1)),
+            dma((2, ns - 1)),
+            dma((ns, nf - 1)),
+            dma((ns, nf - 1)),
+            dma((ns, nf)),
+            dma((ns, nf)),
+        ],
+        compiler_params=pltpu.CompilerParams(
+            collective_id=0, has_side_effects=True, vmem_limit_bytes=50 * 1024 * 1024
+        ),
+    )(act, gain, *weights, gate_weights, w_out_conv, w_out_mem)
+
+
+def output_kernel(nf, mix_ref, wo_ref, out_ref, got, wbuf, acc, w_sem, send, recv, own_sem):
+    sp, fs, tp = (lax.axis_index("sp"), lax.axis_index("fs"), lax.axis_index("tp"))
+    group = nf * 2
+    g = fs * 2 + tp
+    loads = [
+        pltpu.make_async_copy(wo_ref.at[pl.ds(i * 2, 2)], wbuf.at[pl.ds(i * 2, 2)], w_sem.at[i])
+        for i in range(nf)
+    ]
+    for load in loads:
+        load.start()
+    own = pltpu.make_async_copy(mix_ref.at[g], got.at[g], own_sem)
+    own.start()
+
+    def peer(off):
+        to = lax.rem(g + off, group)
+        return (sp, to // 2, lax.rem(to, 2))
+
+    greet([(None, peer(off)) for off in range(1, group)])
+
+    def copy(off, to, source):
+        return pltpu.make_async_remote_copy(
+            mix_ref.at[to],
+            got.at[source],
+            send.at[off - 1],
+            recv.at[off - 1],
+            device_id=peer(off),
+            device_id_type=MESH,
+        )
+
+    for off in range(1, group):
+        copy(off, lax.rem(g + off, group), g).start()
+    for load in loads:
+        load.wait()
+    own.wait()
+
+    def add(source, first):
+        part = jnp.dot(
+            got[source, 0], wbuf[source, 0], preferred_element_type=jnp.float32
+        ) + jnp.dot(got[source, 1], wbuf[source, 1], preferred_element_type=jnp.float32)
+        acc[...] = part if first else acc[...] + part
+
+    add(g, True)
+    for off in range(1, group):
+        source = lax.rem(g + group - off, group)
+        copy(off, lax.rem(g + off, group), source).wait_recv()
+        add(source, False)
+    out_ref[...] = acc[...].astype(jnp.bfloat16)
+    for off in range(1, group):
+        copy(off, lax.rem(g + off, group), g).wait_send()
+
+
+def exchange_and_merge(mix, wo):
+    nf = lax.axis_size("fs")
+    group, _, tokens, channels = mix.shape
+    width = wo.shape[3]
+    vmem = pl.BlockSpec(memory_space=pltpu.VMEM)
+    dma = pltpu.SemaphoreType.DMA
+    return pl.pallas_call(
+        functools.partial(output_kernel, nf),
+        out_shape=jax.ShapeDtypeStruct((tokens, width), jnp.bfloat16),
+        in_specs=[vmem, pl.BlockSpec(memory_space=pl.ANY)],
+        out_specs=vmem,
+        scratch_shapes=[
+            pltpu.VMEM(mix.shape, jnp.bfloat16),
+            pltpu.VMEM(wo.shape, jnp.bfloat16),
+            pltpu.VMEM((tokens, width), jnp.float32),
+            dma((nf,)),
+            dma((group - 1,)),
+            dma((group - 1,)),
+            dma,
+        ],
+        compiler_params=pltpu.CompilerParams(
+            collective_id=1, has_side_effects=True, vmem_limit_bytes=40 * 1024 * 1024
+        ),
+    )(mix, wo)
 
 
 def shards(
@@ -143,31 +578,64 @@
     group_index = lax.axis_index(("fs", "tp"))
     heads_here = MEMORY_HEADS // (lax.axis_size("fs") * lax.axis_size("tp"))
     channels = w_conv_gate.shape[1]
-    sequences = lax.all_gather(activations, "fs", axis=0, tiled=True)
-    seq_count = sequences.shape[0]
-    tokens = sequences.shape[1]
-    model_width = sequences.shape[2]
-    row_count = seq_count * tokens
-    flat_rows = sequences.reshape(row_count, model_width).astype(jnp.float32)
-    normed = (
-        flat_rows
-        * lax.rsqrt(jnp.mean(flat_rows * flat_rows, axis=-1, keepdims=True) + EPSILON)
-        * norm_gain
-    ).astype(jnp.bfloat16)
-    pieces = (
-        lax.all_gather(w_conv_gate, "sp", axis=0, tiled=True),
-        lax.all_gather(w_conv_mult, "sp", axis=0, tiled=True),
-        lax.all_gather(w_conv_in, "sp", axis=0, tiled=True),
-        lax.all_gather(w_query, "sp", axis=0, tiled=True),
-        lax.all_gather(w_key, "sp", axis=0, tiled=True),
-        lax.all_gather(w_value, "sp", axis=0, tiled=True),
-    )
-    projected = tuple(
-        (jnp.dot(normed, shard_piece, preferred_element_type=jnp.float32) for shard_piece in pieces)
-    )
-    conv_gate, conv_mult, conv_in, query, keys_proj, value = [
-        tensor.astype(jnp.bfloat16).reshape(seq_count, tokens, -1) for tensor in projected
-    ]
+    if lax.axis_size("sp") <= 8 and lax.axis_size("tp") == 2:
+        seq_count, tokens = lax.axis_size("fs"), activations.shape[1]
+        all_gates = jnp.concatenate([w_input_gate, w_forget_gate], axis=1)
+        flat, gate_flat, full_out = gather_and_project(
+            activations[0],
+            norm_gain[None, :],
+            (w_conv_gate, w_conv_mult, w_conv_in, w_query, w_key, w_value),
+            all_gates,
+            w_out_conv,
+            w_out_mem,
+        )
+        conv_gate, conv_mult, conv_in, query, keys_proj, value = [
+            flat[:, at * channels : (at + 1) * channels].reshape(seq_count, tokens, channels)
+            for at in range(6)
+        ]
+        gate_values = jnp.concatenate(
+            [
+                lax.dynamic_slice_in_dim(
+                    gate_flat, at + group_index * heads_here, heads_here, 1
+                )
+                for at in (0, MEMORY_HEADS)
+            ],
+            axis=1,
+        ).reshape(seq_count, tokens, 2 * heads_here)
+    else:
+        full_out = None
+        sequences = lax.all_gather(activations, "fs", axis=0, tiled=True)
+        seq_count = sequences.shape[0]
+        tokens = sequences.shape[1]
+        model_width = sequences.shape[2]
+        row_count = seq_count * tokens
+        flat_rows = sequences.reshape(row_count, model_width).astype(jnp.float32)
+        normed = (
+            flat_rows
+            * lax.rsqrt(jnp.mean(flat_rows * flat_rows, axis=-1, keepdims=True) + EPSILON)
+            * norm_gain
+        ).astype(jnp.bfloat16)
+        pieces = (
+            lax.all_gather(w_conv_gate, "sp", axis=0, tiled=True),
+            lax.all_gather(w_conv_mult, "sp", axis=0, tiled=True),
+            lax.all_gather(w_conv_in, "sp", axis=0, tiled=True),
+            lax.all_gather(w_query, "sp", axis=0, tiled=True),
+            lax.all_gather(w_key, "sp", axis=0, tiled=True),
+            lax.all_gather(w_value, "sp", axis=0, tiled=True),
+        )
+        projected = tuple(
+            (jnp.dot(normed, shard_piece, preferred_element_type=jnp.float32) for shard_piece in pieces)
+        )
+        conv_gate, conv_mult, conv_in, query, keys_proj, value = [
+            tensor.astype(jnp.bfloat16).reshape(seq_count, tokens, -1) for tensor in projected
+        ]
+        entry_cols = lax.dynamic_slice_in_dim(w_input_gate, group_index * heads_here, heads_here, 1)
+        forget_cols = lax.dynamic_slice_in_dim(w_forget_gate, group_index * heads_here, heads_here, 1)
+        gate_values = jnp.dot(
+            normed,
+            jnp.concatenate([entry_cols, forget_cols], axis=1),
+            preferred_element_type=jnp.float32,
+        ).reshape(seq_count, tokens, 2 * heads_here)
     product = (conv_mult.astype(jnp.float32) * conv_in.astype(jnp.float32)).astype(jnp.bfloat16)
     ntaps = conv_taps.shape[0]
     rim_rows = from_behind(product[:, tokens - (ntaps - 1) :, :], "sp", 1)
@@ -179,13 +647,6 @@
             mixed_sum + tap_weights[tap_index] * padded[:, tap_index : tap_index + tokens, :]
         )
     conv_out = (conv_gate.astype(jnp.float32) * mixed_sum).astype(jnp.bfloat16)
-    entry_cols = lax.dynamic_slice_in_dim(w_input_gate, group_index * heads_here, heads_here, 1)
-    forget_cols = lax.dynamic_slice_in_dim(w_forget_gate, group_index * heads_here, heads_here, 1)
-    gate_values = jnp.dot(
-        normed,
-        jnp.concatenate([entry_cols, forget_cols], axis=1),
-        preferred_element_type=jnp.float32,
-    ).reshape(seq_count, tokens, 2 * heads_here)
     bias_rows = lax.dynamic_slice_in_dim(gate_bias, group_index * heads_here, heads_here, 1)
     decay_rows = lax.dynamic_slice_in_dim(decay_shift, group_index * heads_here, heads_here, 2)
     entry = gate_values[..., :heads_here] + bias_rows[0]
@@ -207,6 +668,10 @@
         .reshape(seq_count, tokens, heads_here * HEAD_DIM)
         .astype(jnp.bfloat16)
     )
+    if full_out is not None:
+        mix = jnp.stack([conv_out, mem_out]).reshape(2, seq_count * 2, tokens // 2, channels)
+        merged = exchange_and_merge(mix.transpose(1, 0, 2, 3), full_out)
+        return merged[None]
     conv_seq, mem_seq = (
         lax.all_to_all(conv_out, "fs", split_axis=0, concat_axis=2, tiled=True),
         lax.all_to_all(mem_out, "fs", split_axis=0, concat_axis=2, tiled=True),

time: 251 us -> 178 us (0.71)
  blocking collectives: 129 us -> 9 us
  Pallas kernels: 0 us -> 102 us
  waiting for transfers between devices: 48.8 us -> 13.4 us
  matrix products: 24 us -> 4.21 us
  local copies, waits for them, and re-layouts: 6.76 us -> 20.5 us
  starting transfers between devices: 10.1 us -> 1.29 us
  other arithmetic: 16.5 us -> 12.8 us
    all_gather x8 -> x0, blocking collectives: 122 us -> none  [the longest x1 20.7 us: shards(): lax.all_gather(w_conv_in, 'sp', axis=0, tiled=True)]
    pallas_call x0 -> x2, Pallas kernels: none -> 102 us  [the longest x1 89.7 us: gather_and_project(): pl.pallas_call(functools.partial(gather_kernel, ns, nf, cuts), out_shape=...]
    all_gather x3 -> x0, waiting for transfers between devices: 37.1 us -> none  [the longest x1 26.5 us: shards(): sequences = lax.all_gather(activations, 'fs', axis=0, tiled=True)]
    dot_general x9 -> x0, matrix products: 19.8 us -> none  [the longest x6 12.9 us: shards(): jnp.dot(normed, shard_piece, preferred_element_type=jnp.float32)]
    unnamed x28 -> x44, local copies, waits for them, and re-layouts: 2.14 us -> 15.9 us
    all_gather x1, waiting for transfers between devices: 0.02 us -> 13.4 us  [prefix(): pieces = jax.tree.map(lambda part: lax.all_gather(part, axis), value)]
    reduce_scatter x1 -> x0, waiting for transfers between devices: 10.8 us -> none  [shards(): lax.psum_scatter((jnp.dot(conv_flat, full_conv, preferred_element_type=jn...]
    all_to_all x2 -> x0, starting transfers between devices: 6.95 us -> none  [the longest x1 3.55 us: shards(): lax.all_to_all(mem_out, 'fs', split_axis=0, concat_axis=2, tiled=True)]
  transfers between devices with their start and end apart: 8 -> 2, of which waited for: 3 -> 1; matrix products, arithmetic and copies ran while one was open for 10% -> 2% of each run, Pallas kernels for 0% -> 0%
where the time goes in v1:
time: 178 us
  Pallas kernels  102 us (57%)
  local copies, waits for them, and re-layouts  20.5 us (12%)
  between operations  14.4 us (8%)
  waiting for transfers between devices  13.4 us (8%)
  other arithmetic  12.8 us (7%)
  blocking collectives  9 us (5%)
  matrix products  4.21 us (2%)
    pallas_call x1, Pallas kernels, gather_and_project(): pl.pallas_call(functools.partial(gather_kernel, ns, nf, cuts), out_shape=...  89.7 us
    unnamed x44, local copies, waits for them, and re-layouts  15.9 us
    all_gather x1, waiting for transfers between devices, prefix(): pieces = jax.tree.map(lambda part: lax.all_gather(part, axis), value)  13.4 us
    pallas_call x1, Pallas kernels, exchange_and_merge(): pl.pallas_call(functools.partial(output_kernel, nf), out_shape=jax.ShapeD...  12.1 us
    unnamed x1, blocking collectives  9 us
  transfers between devices with their start and end apart: 2, of which 1 were waited for; matrix products, arithmetic and copies ran while one was open for 2% of the time, Pallas kernels for 0%

profile of v1, /device:TPU:1, one launch (start us, length us, event | category | flops | bytes accessed | tf_op | source)
XLA Modules:
  0.0 177.6 jit_solution(4798123181702592818)
XLA Ops:
  6.5 0.8 pad_maximum_fusion
  7.3 0.3 copy.34.wg_ref
  7.6 1.2 copy-done.2
  8.8 0.9 copy-done.3
  9.7 0.9 copy-done.4
  10.7 0.9 copy-done.5
  11.6 0.9 copy-done.6
  12.5 0.9 copy-done.7
  13.4 0.9 copy-done.8
  14.3 0.9 copy-done.9
  15.2 0.9 copy-done.10
  16.1 0.7 copy-done.11
  16.8 89.7 %shard_map.154 = (bf16[1024,768]{1,0:T(8,128)(2,1)}, f32[1024,16]{1,0:T(8,128)S(1)}, bf16[8,2,128,2048]{3,2,1,0:T(8,128)(2,1)}) custom-call(bf16[256,2048]{1,0:T(8,128)(2,1)S(1)} %bitcast.122, f32[1,2048]{1,0:T(1,128)S(1)} %bitcast.123, bf16[512,128]{1,0:T(8,128)(2,1)S(1)} %copy-done.3, bf16[512,128]{1,0:T(8,128)(2,1)S(1)} %copy-done.4, ...), custom_call_target="tpu_custom_call" | custom-call | tf_op jit(solution)/shard_map/pallas_call | solution.py:449
  106.5 1.3 fusion.33
  107.8 0.4 copy-done.13
  108.1 0.8 multiply_convert_fusion.1
  109.0 0.3 constant_dynamic-slice_fusion.6
  109.3 0.2 copy.35
  109.5 0.2 copy.36
  109.8 0.5 fusion.34
  110.4 0.6 slice_add_fusion
  111.1 1.4 fusion.27
  112.4 0.1 reshape_reshape_transpose.6
  112.5 0.9 reduce_window_sum.11
  113.5 0.2 slice_reduce_fusion
  113.6 0.2 fusion.30
  113.9 0.1 copy.39
  114.0 0.1 copy.38
  114.1 2.0 %convolution_bitcast_fusion = f32[4,4,128,128]{3,2,0,1:T(8,128)S(1)} fusion(f32[4,4,64,128]{3,2,1,0:T(8,128)S(1)} %bitcast.124, bf16[4,4,64,128]{3,2,1,0:T(8,128)(2,1)S(1)} %bitcast.126, f32[4,4,64]{2,1,0:T(4,128)S(1)} %subtract_exponential_fusion.5), kind=kOutput, calls=%fused_computation.30 | convolution fusion | flops 201588736 | bytes 1839104 | tf_op jit(solution)/shard_map/bclv,bclk->bcvk/dot_general | solution.py:79
  116.1 3.9 %while.39 = (s32[]{:T(128)}, f32[4]{0:T(128)S(1)}, f32[4]{0:T(128)S(1)}, f32[4,128,128]{2,1,0:T(8,128)S(1)}, f32[4,4]{1,0:T(4,128)S(1)}, /*index=5*/f32[4,4]{1,0...) while((s32[]{:T(128)}, f32[4]{0:T(128)S(1)}, ...), condition=%wide.region_3.4_spmd.clone, body=%wide.region_2.3_spmd.clone.sunk | while | flops 327711 | bytes 1311669 | solution.py:97
  116.1 0.7 bitcast_dynamic-update-slice_fusion.2
  116.9 0.1 fusion.46
  117.1 0.7 bitcast_dynamic-update-slice_fusion.2
  117.9 0.1 fusion.46
  118.1 0.7 bitcast_dynamic-update-slice_fusion.2
  118.8 0.1 fusion.46
  119.0 0.7 bitcast_dynamic-update-slice_fusion.2
  119.8 0.1 fusion.46
  120.0 0.7 copy-done.12
  120.7 1.3 collective-permute-start
  122.1 0.4 fusion.20
  122.5 0.7 dynamic-slice
  123.9 0.2 dynamic-update-slice
  124.1 0.2 dynamic-update-slice.1
  124.3 9.0 %all-reduce.2 = (f32[16]{0:T(128)S(1)}, f32[16]{0:T(128)S(1)}) all-reduce(f32[16]{0:T(128)S(1)} %dynamic-update-slice, f32[16]{0:T(128)S(1)} %dynamic-update-slice.1), channel_id=2, replica_groups=mesh['sp'=4,'fs'=4,'tp'=2] {'sp'}, use_global_device_ids=true, to_apply=%add | all-reduce | flops 32 | bytes 256
  133.3 0.1 reshape.134
  133.5 0.8 dynamic_slice.55
  134.3 0.2 fusion.18
  134.5 13.4 %all-gather.5.cloned.1.call-done = f32[16,128,128]{2,1,0:T(8,128)} async-done(((f32[4,128,128]{2,1,0:T(8,128)}), f32[16,128,128]{2,1,0:T(8,128)}) %all-gather.5.cloned.1.call-update) | async-done | bytes 1048592 | tf_op jit(solution)/shard_map/all_gather | solution.py:22
  147.9 3.4 %while.40 = (s32[]{:T(128)}, f32[4]{0:T(128)S(1)}, f32[4]{0:T(128)S(1)}, f32[4,128,128]{2,1,0:T(8,128)S(1)}, s32[]{:T(128)}, /*index=5*/f32[4,4]{1,0:T(4,128)S(1...) while((s32[]{:T(128)}, f32[4]{0:T(128)S(1)}, f32[4]{0:T(128)S(1)}, ...), condition=%wide.region_5.6_spmd.clone, body=%wide.region_4.5_spmd.clone.sunk | while | flops 327728 | bytes 786793 | solution.py:31
  148.0 1.1 fusion.47
  149.1 1.1 fusion.47
  150.3 1.1 fusion.47
  151.4 0.1 copy.41
  151.5 0.1 subtract_exponential_fusion.4
  151.6 0.6 convolution_multiply_fusion.1
  152.1 0.4 fusion.35
  152.5 0.1 multiply_add_fusion
  152.6 0.2 copy-done.15
  152.8 1.3 multiply_reduce_fusion
  154.2 0.2 multiply_convert_fusion
  154.5 3.4 %copy-done.1 = bf16[8,2,128,2048]{3,2,1,0:T(8,128)(2,1)S(1)} copy-done((bf16[8,2,128,2048]{3,2,1,0:T(8,128)(2,1)S(1)}, bf16[8,2,128,2048]{3,2,1,0:T(8,128)(2,1)}, u32[]{:S(2)}) %copy-start.1) | copy-done | bytes 8388632
  157.9 12.1 %shard_map.155 = bf16[128,2048]{1,0:T(8,128)(2,1)S(1)} custom-call(bf16[8,2,128,128]{3,2,1,0:T(8,128)(2,1)S(1)} %maximum_bitcast_fusion.mix_ref, bf16[8,2,128,2048]{3,2,1,0:T(8,128)(2,1)S(1)} %copy-done.1), custom_call_target="tpu_custom_call" | custom-call | tf_op jit(solution)/shard_map/pallas_call | solution.py:540
  169.9 0.8 copy.88
  (76 shorter events, 1.2 us)
Async XLA Ops:
  6.5 115.5 %copy-start = (f32[3,1024]{1,0:T(4,128)S(1)}, f32[3,1024]{1,0:T(4,128)}, u32[]{:S(2)}) copy-start(f32[3,1024]{1,0:T(4,128)} %param.25) | copy-start | bytes 36868
  6.5 141.4 %all-gather.5.cloned.1.call-start = ((), (), s32[]{:S(2)}) async-start(), calls=%async_computation | async-start | bytes 1310720 | tf_op jit(solution)/shard_map/all_gather | solution.py:22
  7.6 1.2 copy-start.2
  8.8 0.9 copy-start.3
  9.7 0.9 copy-start.4
  10.6 0.9 copy-start.5
  11.6 0.9 copy-start.6
  12.5 0.9 copy-start.7
  13.4 0.9 copy-start.8
  14.3 0.9 copy-start.9
  15.2 0.9 copy-start.10
  16.1 0.7 copy-start.11
  106.5 1.7 copy-start.13
  109.0 0.8 copy-start.16
  116.1 4.6 %copy-start.14 = (bf16[1024,128]{1,0:T(8,128)(2,1)S(1)}, bf16[1024,128]{1,0:T(8,128)(2,1)}, u32[]{:S(2)}) copy-start(bf16[1024,128]{1,0:T(8,128)(2,1)} %get-tuple-element.363) | copy-start | bytes 786436
  116.1 6.5 %copy-start.17 = (u32[32]{0:T(128)S(1)}, u32[32]{0:T(128)}, u32[]{:S(2)}) copy-start(u32[32]{0:T(128)} %constant.88) | copy-start | bytes 388
  120.0 0.7 copy-start.12
  120.7 13.5 %collective-permute-start = (bf16[4,2,128]{2,1,0:T(2,128)(2,1)S(1)}, bf16[4,2,128]{2,1,0:T(2,128)(2,1)S(1)}, u32[]{:S(2)}, u32[]{:S(2)}) collective-permute-start(bf16[4,2,128]{2,1,0:T(2,128)(2,1)S(1)} %slice.72), channel_id=1, source_target_pairs={{0,8},{8,16},{16,24},{1,9},{9,17},{17,25},{2,10},{10,18},{18,26},{... | collective-permute-start | bytes 6152 | tf_op jit(solution)/shard_map/ppermute | solution.py:37
  151.6 1.2 copy-start.15
  154.5 3.4 %copy-start.1 = (bf16[8,2,128,2048]{3,2,1,0:T(8,128)(2,1)S(1)}, bf16[8,2,128,2048]{3,2,1,0:T(8,128)(2,1)}, u32[]{:S(2)}) copy-start(bf16[8,2,128,2048]{3,2,1,0:T(8,128)(2,1)} %get-tuple-element.217.wo_ref) | copy-start | bytes 25165828
Sparse Core Ops, SparseCore 0:
  120.8 27.0 all-gather.4

commit v2 on v1

--- a/solution.py
+++ b/solution.py
@@ -19,7 +19,13 @@
 
 def prefix(value, axis, join, neutral):
     count, mine = (lax.axis_size(axis), lax.axis_index(axis))
-    pieces = jax.tree.map(lambda part: lax.all_gather(part, axis), value)
+    total, peak, state = value
+    stats = jnp.stack([total, peak], axis=1)[..., None]
+    stats = jnp.broadcast_to(stats, stats.shape[:2] + state.shape[-1:])
+    stats = jnp.pad(stats, ((0, 0), (0, 6), (0, 0)))
+    packed = lax.all_gather(jnp.concatenate([state, stats], axis=1), axis)
+    height = state.shape[1]
+    pieces = (packed[:, :, height, 0], packed[:, :, height + 1, 0], packed[:, :, :height])
     subtotal = jax.tree.map(
         lambda part, zero: jnp.full_like(part, 0) + jnp.asarray(zero, part.dtype), value, neutral
     )
@@ -28,6 +34,10 @@
         longer = join(subtotal, jax.tree.map(lambda part: part[position], pieces))
         return jax.tree.map(lambda new, old: jnp.where(position < mine, new, old), longer, subtotal)
 
+    if count <= 8:
+        for position in range(count - 1):
+            subtotal = lap(position, subtotal)
+        return subtotal
     return lax.fori_loop(0, count - 1, lap, subtotal)
 
 
@@ -380,32 +390,6 @@
 
     lax.fori_loop(0, nf, gates, 0)
 
-    for d in range(1, ns):
-        for k in range(cuts):
-            for side in range(2):
-
-                @pl.when(arrives(side, d))
-                def _():
-                    w_copy(side, d - 1, owner_of(side, d), k).wait_recv()
-                    if d < ns - 1:
-                        send_w(side, d, k)
-
-        for side in range(2):
-
-            @pl.when(arrives(side, d))
-            def _():
-                multiply(owner_of(side, d), False)
-
-        if d + 1 < ns:
-            z_round(d + 1)
-
-    def round_rows(i, carry):
-        here = pl.ds(pl.multiple_of(i * tile, tile), tile)
-        proj_ref[here, :] = total[here, :].astype(jnp.bfloat16)
-        return carry
-
-    lax.fori_loop(0, nf, round_rows, 0)
-
     def collect(s, carry):
         for off in range(1, nf):
             src_g = origin(off) * 2 + tp
@@ -413,7 +397,33 @@
             d_copy(s, off, src_g).start()
         return carry
 
-    lax.fori_loop(0, ns, collect, 0)
+    for d in range(1, ns):
+        if d == ns - 1:
+            lax.fori_loop(0, ns, collect, 0)
+        for k in range(cuts):
+            for side in range(2):
+
+                @pl.when(arrives(side, d))
+                def _():
+                    w_copy(side, d - 1, owner_of(side, d), k).wait_recv()
+                    if d < ns - 1:
+                        send_w(side, d, k)
+
+        for side in range(2):
+
+            @pl.when(arrives(side, d))
+            def _():
+                multiply(owner_of(side, d), False)
+
+        if d + 1 < ns:
+            z_round(d + 1)
+
+    def round_rows(i, carry):
+        here = pl.ds(pl.multiple_of(i * tile, tile), tile)
+        proj_ref[here, :] = total[here, :].astype(jnp.bfloat16)
+        return carry
+
+    lax.fori_loop(0, nf, round_rows, 0)
 
     def finish(s, carry):
         for off in range(nf):
@@ -445,6 +455,7 @@
     count = nf * tokens
     cuts = 2
     vmem = pl.BlockSpec(memory_space=pltpu.VMEM)
+    hbm = pl.BlockSpec(memory_space=pltpu.MemorySpace.HBM)
     dma = pltpu.SemaphoreType.DMA
     return pl.pallas_call(
         functools.partial(gather_kernel, ns, nf, cuts),
@@ -453,7 +464,7 @@
             jax.ShapeDtypeStruct((count, gate_weights.shape[1]), jnp.float32),
             jax.ShapeDtypeStruct((nf * 2, 2, rows, ns * ocols), jnp.bfloat16),
         ),
-        in_specs=[vmem] * 11,
+        in_specs=[hbm, vmem] + [hbm] * 6 + [vmem, hbm, hbm],
         out_specs=(vmem, vmem, pl.BlockSpec(memory_space=pl.ANY)),
         scratch_shapes=[
             pltpu.VMEM((nf, tokens, model), jnp.bfloat16),
@@ -540,7 +551,7 @@
     return pl.pallas_call(
         functools.partial(output_kernel, nf),
         out_shape=jax.ShapeDtypeStruct((tokens, width), jnp.bfloat16),
-        in_specs=[vmem, pl.BlockSpec(memory_space=pl.ANY)],
+        in_specs=[vmem, pl.BlockSpec(memory_space=pltpu.MemorySpace.HBM)],
         out_specs=vmem,
         scratch_shapes=[
             pltpu.VMEM(mix.shape, jnp.bfloat16),

time: 178 us -> 172 us (0.966)
  waiting for transfers between devices: 13.4 us -> 25.8 us
  blocking collectives: 9 us -> 0 us
  Pallas kernels: 102 us -> 96.3 us
  other arithmetic: 12.8 us -> 9.72 us
    all_gather x1, waiting for transfers between devices: 13.4 us -> 25.8 us  [prefix(): packed = lax.all_gather(jnp.concatenate([state, stats], axis=1), axis)]
    unnamed x1 -> x0, blocking collectives: 9 us -> none
    pallas_call x1, Pallas kernels: 89.7 us -> 84.1 us  [gather_and_project(): pl.pallas_call(functools.partial(gather_kernel, ns, nf, cuts), out_shape=...]
    select_n x3 -> x0, other arithmetic: 3.21 us -> none  [lap(): jnp.where(position < mine, new, old)]
    unnamed x44 -> x41, local copies, waits for them, and re-layouts: 15.9 us -> 14.5 us
  transfers between devices with their start and end apart: 2 -> 2, of which waited for: 1 -> 1; matrix products, arithmetic and copies ran while one was open for 2% -> 1% of each run, Pallas kernels for 0% -> 0%
where the time goes in v2:
time: 172 us; the launch traced here: 171 us
  Pallas kernels  96.3 us (56%)
  waiting for transfers between devices  25.8 us (15%)
  local copies, waits for them, and re-layouts  20 us (12%)
  between operations  13.7 us (8%)
  other arithmetic  9.72 us (6%)
  matrix products  4.22 us (2%)
    pallas_call x1, Pallas kernels, gather_and_project(): pl.pallas_call(functools.partial(gather_kernel, ns, nf, cuts), out_shape=...  84.1 us
    all_gather x1, waiting for transfers between devices, prefix(): packed = lax.all_gather(jnp.concatenate([state, stats], axis=1), axis)  25.8 us
    unnamed x41, local copies, waits for them, and re-layouts  14.5 us
    pallas_call x1, Pallas kernels, exchange_and_merge(): pl.pallas_call(functools.partial(output_kernel, nf), out_shape=jax.ShapeD...  12.1 us
  transfers between devices with their start and end apart: 2, of which 1 were waited for; matrix products, arithmetic and copies ran while one was open for 1% of the time, Pallas kernels for 0%

profile of v2, /device:TPU:1, one launch (start us, length us, event | category | flops | bytes accessed | tf_op | source)
XLA Modules:
  0.0 171.3 jit_solution(5176560814979547412)
XLA Ops:
  6.6 0.8 pad_maximum_fusion
  7.3 0.3 copy.48.wg_ref
  7.6 1.2 copy-done.2
  8.9 0.9 copy-done.3
  9.8 0.9 copy-done.4
  10.7 0.9 copy-done.5
  11.6 0.9 copy-done.6
  12.5 0.9 copy-done.7
  13.4 0.9 copy-done.8
  14.3 0.9 copy-done.9
  15.2 0.9 copy-done.10
  16.1 0.7 copy-done.11
  16.8 84.1 %shard_map.154 = (bf16[1024,768]{1,0:T(8,128)(2,1)}, f32[1024,16]{1,0:T(8,128)S(1)}, bf16[8,2,128,2048]{3,2,1,0:T(8,128)(2,1)}) custom-call(bf16[256,2048]{1,0:T(8,128)(2,1)S(1)} %bitcast.210, f32[1,2048]{1,0:T(1,128)S(1)} %bitcast.211, bf16[512,128]{1,0:T(8,128)(2,1)S(1)} %copy-done.3, bf16[512,128]{1,0:T(8,128)(2,1)S(1)} %copy-done.4, ...), custom_call_target="tpu_custom_call" | custom-call | tf_op jit(solution)/shard_map/pallas_call | solution.py:460
  100.9 1.3 fusion.44
  102.2 0.4 copy-done.12
  102.6 0.1 multiply_convert_fusion.1
  102.8 0.5 fusion.46
  103.3 0.3 constant_dynamic-slice_fusion.4
  103.6 0.2 copy.49
  103.8 0.2 copy.50
  104.1 1.5 fusion.33
  105.5 0.1 reshape_reshape_transpose.6
  105.6 0.9 reduce_window_sum.11
  106.6 0.2 slice_reduce_fusion
  106.7 0.1 copy.52
  106.8 0.6 slice_add_fusion
  107.5 0.1 reshape_reshape_transpose.7
  107.5 0.2 fusion.36
  107.7 0.1 subtract_exponential_fusion.3
  107.8 0.1 copy.53
  107.9 2.0 %convolution_bitcast_fusion = f32[4,4,128,128]{3,2,0,1:T(8,128)S(1)} fusion(f32[4,4,64,128]{3,2,1,0:T(8,128)S(1)} %bitcast.212, bf16[4,4,64,128]{3,2,1,0:T(8,128)(2,1)S(1)} %bitcast.214, f32[4,4,64]{2,1,0:T(4,128)S(1)} %subtract_exponential_fusion.3), kind=kOutput, calls=%fused_computation.16 | convolution fusion | flops 201588736 | bytes 1839104 | tf_op jit(solution)/shard_map/bclv,bclk->bcvk/dot_general | solution.py:89
  109.9 3.9 %while.21 = (s32[]{:T(128)}, f32[4]{0:T(128)S(1)}, f32[4]{0:T(128)S(1)}, f32[4,128,128]{2,1,0:T(8,128)S(1)}, f32[4,4]{1,0:T(4,128)S(1)}, /*index=5*/f32[4,4]{1,0...) while((s32[]{:T(128)}, f32[4]{0:T(128)S(1)}, ...), condition=%wide.region_3.4_spmd.clone, body=%wide.region_2.3_spmd.clone.sunk | while | flops 327711 | bytes 1311169 | solution.py:107
  110.0 0.7 bitcast_dynamic-update-slice_fusion.2
  110.7 0.1 fusion.57
  111.0 0.8 bitcast_dynamic-update-slice_fusion.2
  111.7 0.1 fusion.57
  112.0 0.8 bitcast_dynamic-update-slice_fusion.2
  112.7 0.1 fusion.57
  113.0 0.7 bitcast_dynamic-update-slice_fusion.2
  113.7 0.1 fusion.57
  113.8 0.1 copy.55
  114.0 0.7 select_maximum_fusion
  114.8 1.5 collective-permute-start
  116.3 0.4 fusion.15
  116.7 0.8 dynamic_slice.34
  117.5 0.2 fusion.13
  117.8 25.8 %all-gather.3.cloned.1.call-done = f32[16,136,128]{2,1,0:T(8,128)} async-done(((f32[4,136,128]{2,1,0:T(8,128)}), f32[16,136,128]{2,1,0:T(8,128)}) %all-gather.3.cloned.1.call-update) | async-done | bytes 1114128 | tf_op jit(solution)/shard_map/all_gather | solution.py:26
  143.5 0.9 fusion.45
  144.4 0.1 copy.68
  144.5 0.1 copy.67
  144.6 0.1 copy.70
  144.7 0.1 copy.66
  144.8 0.1 copy.65
  144.9 0.1 copy.69
  145.0 0.1 copy.62
  145.1 0.1 subtract_exponential_fusion.2
  145.2 0.6 convolution_multiply_fusion.1
  145.8 0.4 fusion.47
  146.2 0.2 fusion.22
  146.5 1.3 multiply_reduce_fusion
  147.8 0.2 multiply_convert_fusion
  148.1 3.4 %copy-done.1 = bf16[8,2,128,2048]{3,2,1,0:T(8,128)(2,1)S(1)} copy-done((bf16[8,2,128,2048]{3,2,1,0:T(8,128)(2,1)S(1)}, bf16[8,2,128,2048]{3,2,1,0:T(8,128)(2,1)}, u32[]{:S(2)}) %copy-start.1) | copy-done | bytes 8388632
  151.5 12.1 %shard_map.155 = bf16[128,2048]{1,0:T(8,128)(2,1)S(1)} custom-call(bf16[8,2,128,128]{3,2,1,0:T(8,128)(2,1)S(1)} %maximum_bitcast_fusion.mix_ref, bf16[8,2,128,2048]{3,2,1,0:T(8,128)(2,1)S(1)} %copy-done.1), custom_call_target="tpu_custom_call" | custom-call | tf_op jit(solution)/shard_map/pallas_call | solution.py:551
  163.7 0.8 copy.100
  (62 shorter events, 1.0 us)
Async XLA Ops:
  6.5 109.7 %copy-start = (f32[3,1024]{1,0:T(4,128)S(1)}, f32[3,1024]{1,0:T(4,128)}, u32[]{:S(2)}) copy-start(f32[3,1024]{1,0:T(4,128)} %param.23) | copy-start | bytes 36868
  6.5 137.0 %all-gather.3.cloned.1.call-start = ((), (), s32[]{:S(2)}) async-start(), calls=%async_computation | async-start | bytes 1392640 | tf_op jit(solution)/shard_map/all_gather | solution.py:26
  7.6 1.2 copy-start.2
  8.9 0.9 copy-start.3
  9.8 0.9 copy-start.4
  10.7 0.9 copy-start.5
  11.6 0.9 copy-start.6
  12.5 0.9 copy-start.7
  13.4 0.9 copy-start.8
  14.3 0.9 copy-start.9
  15.2 0.9 copy-start.10
  16.1 0.7 copy-start.11
  100.9 1.7 copy-start.12
  100.9 1.8 %copy-start.15 = (f32[2,8]{1,0:T(2,128)S(1)}, f32[2,8]{1,0:T(2,128)}, u32[]{:S(2)}) copy-start(f32[2,8]{1,0:T(2,128)} %param.29) | copy-start | bytes 196
  114.8 2.7 %collective-permute-start = (bf16[4,2,128]{2,1,0:T(2,128)(2,1)S(1)}, bf16[4,2,128]{2,1,0:T(2,128)(2,1)S(1)}, u32[]{:S(2)}, u32[]{:S(2)}) collective-permute-start(bf16[4,2,128]{2,1,0:T(2,128)(2,1)S(1)} %slice.126), channel_id=1, source_target_pairs={{0,8},{8,16},{16,24},{1,9},{9,17},{17,25},{2,10},{10,18},{18,26},{... | collective-permute-start | bytes 6152 | tf_op jit(solution)/shard_map/ppermute | solution.py:47
  143.5 2.7 %copy-start.14 = (f32[16,136,128]{2,1,0:T(8,128)S(1)}, f32[16,136,128]{2,1,0:T(8,128)}, u32[]{:S(2)}) copy-start(f32[16,136,128]{2,1,0:T(8,128)} %all-gather.3.cloned.1.call-done) | copy-start | bytes 3342340
  145.2 1.2 copy-start.13
  148.1 3.4 %copy-start.1 = (bf16[8,2,128,2048]{3,2,1,0:T(8,128)(2,1)S(1)}, bf16[8,2,128,2048]{3,2,1,0:T(8,128)(2,1)}, u32[]{:S(2)}) copy-start(bf16[8,2,128,2048]{3,2,1,0:T(8,128)(2,1)} %get-tuple-element.73.wo_ref) | copy-start | bytes 25165828
Sparse Core Ops, SparseCore 0:
  114.9 28.6 all-gather.2

commit v3 on v2

--- a/solution.py
+++ b/solution.py
@@ -17,15 +17,73 @@
 HIGHEST_PRECISION = lax.Precision.HIGHEST
 
 
+def later_kernel(ns, state_ref, stat_ref, states, stats, s_send, s_recv, t_send, t_recv):
+    sp, fs, tp = (lax.axis_index("sp"), lax.axis_index("fs"), lax.axis_index("tp"))
+    greet([(None, (lax.rem(sp + off, ns), fs, tp)) for off in range(1, ns)])
+
+    def copies(off, source):
+        to = (sp + off, fs, tp)
+        return (
+            pltpu.make_async_remote_copy(
+                stat_ref, stats.at[source], t_send.at[off - 1], t_recv.at[off - 1],
+                device_id=to, device_id_type=MESH,
+            ),
+            pltpu.make_async_remote_copy(
+                state_ref, states.at[source], s_send.at[off - 1], s_recv.at[off - 1],
+                device_id=to, device_id_type=MESH,
+            ),
+        )
+
+    for off in range(1, ns):
+
+        @pl.when(sp + off < ns)
+        def _():
+            for copy in copies(off, sp):
+                copy.start()
+
+    for off in range(1, ns):
+
+        @pl.when(sp - off >= 0)
+        def _():
+            for copy in copies(off, sp - off):
+                copy.wait_recv()
+
+    for off in range(1, ns):
+
+        @pl.when(sp + off < ns)
+        def _():
+            for copy in copies(off, sp):
+                copy.wait_send()
+
+
+def send_later(state, stats, ns):
+    vmem = pl.BlockSpec(memory_space=pltpu.VMEM)
+    return pl.pallas_call(
+        functools.partial(later_kernel, ns),
+        out_shape=(
+            jax.ShapeDtypeStruct((ns,) + state.shape, state.dtype),
+            jax.ShapeDtypeStruct((ns,) + stats.shape, stats.dtype),
+        ),
+        in_specs=[vmem, vmem],
+        out_specs=(vmem, vmem),
+        scratch_shapes=[pltpu.SemaphoreType.DMA((ns - 1,))] * 4,
+        compiler_params=pltpu.CompilerParams(collective_id=2, has_side_effects=True),
+    )(state, stats)
+
+
 def prefix(value, axis, join, neutral):
     count, mine = (lax.axis_size(axis), lax.axis_index(axis))
     total, peak, state = value
     stats = jnp.stack([total, peak], axis=1)[..., None]
     stats = jnp.broadcast_to(stats, stats.shape[:2] + state.shape[-1:])
     stats = jnp.pad(stats, ((0, 0), (0, 6), (0, 0)))
-    packed = lax.all_gather(jnp.concatenate([state, stats], axis=1), axis)
-    height = state.shape[1]
-    pieces = (packed[:, :, height, 0], packed[:, :, height + 1, 0], packed[:, :, :height])
+    if count <= 8:
+        states, stats = send_later(state.astype(jnp.bfloat16), stats, count)
+        pieces = (stats[:, :, 0, 0], stats[:, :, 1, 0], states.astype(jnp.float32))
+    else:
+        packed = lax.all_gather(jnp.concatenate([state, stats], axis=1), axis)
+        height = state.shape[1]
+        pieces = (packed[:, :, height, 0], packed[:, :, height + 1, 0], packed[:, :, :height])
     subtotal = jax.tree.map(
         lambda part, zero: jnp.full_like(part, 0) + jnp.asarray(zero, part.dtype), value, neutral
     )

time: 172 us -> 152 us (0.88); the launches traced: 171 us -> 149 us
  waiting for transfers between devices: 25.8 us -> 0.01 us
  Pallas kernels: 96.3 us -> 112 us
  between operations: 13.7 us -> 0.4 us
  other arithmetic: 9.72 us -> 11.9 us
    all_gather x1 -> x0, waiting for transfers between devices: 25.8 us -> none  [prefix(): packed = lax.all_gather(jnp.concatenate([state, stats], axis=1), axis)]
    pallas_call x0 -> x1, Pallas kernels: none -> 14.6 us  [send_later(): pl.pallas_call(functools.partial(later_kernel, ns), out_shape=(jax.ShapeD...]
  transfers between devices with their start and end apart: 2 -> 1, of which waited for: 1 -> 0; matrix products, arithmetic and copies ran while one was open for 1% -> 12% of each run, Pallas kernels for 0% -> 10%
where the time goes in v3:
time: 152 us; the launch traced here: 149 us
  Pallas kernels  112 us (74%)
  local copies, waits for them, and re-layouts  19.2 us (13%)
  other arithmetic  11.9 us (8%)
  matrix products  4.22 us (3%)
    pallas_call x1, Pallas kernels, gather_and_project(): pl.pallas_call(functools.partial(gather_kernel, ns, nf, cuts), out_shape=...  84.1 us
    pallas_call x1, Pallas kernels, send_later(): pl.pallas_call(functools.partial(later_kernel, ns), out_shape=(jax.ShapeD...  14.6 us
    unnamed x41, local copies, waits for them, and re-layouts  14.4 us
    pallas_call x1, Pallas kernels, exchange_and_merge(): pl.pallas_call(functools.partial(output_kernel, nf), out_shape=jax.ShapeD...  13.2 us
  transfers between devices with their start and end apart: 1, of which 0 were waited for; matrix products, arithmetic and copies ran while one was open for 12% of the time, Pallas kernels for 10%

profile of v3, /device:TPU:1, one launch (start us, length us, event | category | flops | bytes accessed | tf_op | source)
XLA Modules:
  0.0 149.2 jit_solution(4424998440761914225)
XLA Ops:
  0.0 0.8 pad_maximum_fusion
  0.8 0.3 copy.36.wg_ref
  1.1 1.2 copy-done.2
  2.3 0.9 copy-done.3
  3.2 0.9 copy-done.4
  4.1 0.9 copy-done.5
  5.0 0.9 copy-done.6
  5.9 0.9 copy-done.7
  6.8 0.9 copy-done.8
  7.7 0.9 copy-done.9
  8.6 0.9 copy-done.10
  9.5 0.7 copy-done.11
  10.2 84.1 %shard_map.154 = (bf16[1024,768]{1,0:T(8,128)(2,1)}, f32[1024,16]{1,0:T(8,128)S(1)}, bf16[8,2,128,2048]{3,2,1,0:T(8,128)(2,1)}) custom-call(bf16[256,2048]{1,0:T(8,128)(2,1)S(1)} %bitcast.127, f32[1,2048]{1,0:T(1,128)S(1)} %bitcast.128, bf16[512,128]{1,0:T(8,128)(2,1)S(1)} %copy-done.3, bf16[512,128]{1,0:T(8,128)(2,1)S(1)} %copy-done.4, ...), custom_call_target="tpu_custom_call" | custom-call | tf_op jit(solution)/shard_map/pallas_call | solution.py:518
  94.4 1.3 multiply_convert_fusion.1
  95.8 1.5 collective-permute-start
  97.4 0.8 fusion.39
  98.2 0.1 constant_dynamic-slice_fusion.2
  98.3 0.5 fusion.40
  98.8 0.3 constant_dynamic-slice_fusion.4
  99.1 0.2 copy.37
  99.3 0.2 copy.38
  99.6 1.4 fusion.33
  101.0 0.1 reshape_reshape_transpose.6
  101.1 0.9 reduce_window_sum.11
  102.0 0.2 slice_reduce_fusion
  102.2 0.1 copy.40
  102.3 0.6 slice_add_fusion
  102.9 0.1 reshape_reshape_transpose.7
  103.0 0.2 fusion.37
  103.1 0.1 subtract_exponential_fusion.3
  103.2 0.1 copy.41
  103.3 2.0 %convolution_bitcast_fusion = f32[4,4,128,128]{3,2,0,1:T(8,128)S(1)} fusion(f32[4,4,64,128]{3,2,1,0:T(8,128)S(1)} %bitcast.129, bf16[4,4,64,128]{3,2,1,0:T(8,128)(2,1)S(1)} %bitcast.131, f32[4,4,64]{2,1,0:T(4,128)S(1)} %subtract_exponential_fusion.3), kind=kOutput, calls=%fused_computation.16 | convolution fusion | flops 201588736 | bytes 1839104 | tf_op jit(solution)/shard_map/bclv,bclk->bcvk/dot_general | solution.py:147
  105.3 3.9 %while.21 = (s32[]{:T(128)}, f32[4]{0:T(128)S(1)}, f32[4]{0:T(128)S(1)}, f32[4,128,128]{2,1,0:T(8,128)S(1)}, f32[4,4]{1,0:T(4,128)S(1)}, /*index=5*/f32[4,4]{1,0...) while((s32[]{:T(128)}, f32[4]{0:T(128)S(1)}, ...), condition=%wide.region_3.4_spmd.clone, body=%wide.region_2.3_spmd.clone.sunk | while | flops 327711 | bytes 1311169 | solution.py:165
  105.4 0.7 bitcast_dynamic-update-slice_fusion.2
  106.2 0.1 fusion.51
  106.4 0.7 bitcast_dynamic-update-slice_fusion.2
  107.1 0.1 fusion.51
  107.4 0.7 bitcast_dynamic-update-slice_fusion.2
  108.1 0.1 fusion.51
  108.4 0.7 bitcast_dynamic-update-slice_fusion.2
  109.1 0.1 fusion.51
  109.2 0.1 copy.43
  109.3 0.1 broadcast_in_dim.32
  109.4 0.6 pad.4.stat_ref
  110.0 0.7 convert_element_type.65.state_ref
  110.7 14.6 %shard_map.155 = (bf16[4,4,128,128]{3,2,1,0:T(8,128)(2,1)}, f32[4,4,8,128]{3,2,1,0:T(8,128)}) custom-call(bf16[4,128,128]{2,1,0:T(8,128)(2,1)} %convert_element_type.65.state_ref, f32[4,8,128]{2,1,0:T(8,128)} %pad.4.stat_ref), custom_call_target="tpu_custom_call" | custom-call | tf_op jit(solution)/shard_map/pallas_call | solution.py:61
  125.3 1.0 slice_reduce_fusion.1
  126.3 0.1 copy.44
  126.4 0.8 dynamic_slice.34
  127.2 0.4 fusion.15
  127.6 0.1 subtract_exponential_fusion.2
  127.7 0.6 convolution_multiply_fusion.1
  128.2 0.4 fusion.41
  128.6 0.1 convert_element_type.66
  128.8 0.2 fusion.22
  129.0 0.9 copy-done.15
  129.9 1.3 multiply_reduce_fusion
  131.2 0.1 rsqrt.12
  131.2 0.2 multiply_convert_fusion
  131.5 0.1 maximum_convert_fusion
  131.6 0.2 fusion.13
  131.9 3.4 %copy-done.1 = bf16[8,2,128,2048]{3,2,1,0:T(8,128)(2,1)S(1)} copy-done((bf16[8,2,128,2048]{3,2,1,0:T(8,128)(2,1)S(1)}, bf16[8,2,128,2048]{3,2,1,0:T(8,128)(2,1)}, u32[]{:S(2)}) %copy-start.1) | copy-done | bytes 8388632
  135.2 13.2 %shard_map.156 = bf16[128,2048]{1,0:T(8,128)(2,1)S(1)} custom-call(bf16[8,2,128,128]{3,2,1,0:T(8,128)(2,1)S(1)} %maximum_bitcast_fusion.mix_ref, bf16[8,2,128,2048]{3,2,1,0:T(8,128)(2,1)S(1)} %copy-done.1), custom_call_target="tpu_custom_call" | custom-call | tf_op jit(solution)/shard_map/pallas_call | solution.py:609
  148.4 0.8 copy.76
  (63 shorter events, 0.7 us)
Async XLA Ops:
  0.0 127.2 %copy-start = (f32[3,1024]{1,0:T(4,128)S(1)}, f32[3,1024]{1,0:T(4,128)}, u32[]{:S(2)}) copy-start(f32[3,1024]{1,0:T(4,128)} %param.23) | copy-start | bytes 36868
  1.1 1.2 copy-start.2
  2.3 0.9 copy-start.3
  3.2 0.9 copy-start.4
  4.1 0.9 copy-start.5
  5.0 0.9 copy-start.6
  5.9 0.9 copy-start.7
  6.8 0.9 copy-start.8
  7.7 0.9 copy-start.9
  8.6 0.9 copy-start.10
  9.5 0.7 copy-start.11
  94.4 3.0 %copy-start.12 = (bf16[1024,768]{1,0:T(8,128)(2,1)S(1)}, bf16[1024,768]{1,0:T(8,128)(2,1)}, u32[]{:S(2)}) copy-start(bf16[1024,768]{1,0:T(8,128)(2,1)} %get-tuple-element.67) | copy-start | bytes 4718596
  94.4 3.8 %copy-start.18 = (f32[2,8]{1,0:T(2,128)S(1)}, f32[2,8]{1,0:T(2,128)}, u32[]{:S(2)}) copy-start(f32[2,8]{1,0:T(2,128)} %param.29) | copy-start | bytes 196
  95.8 1.6 %copy-start.13 = (bf16[1024,128]{1,0:T(8,128)(2,1)}, bf16[1024,128]{1,0:T(8,128)(2,1)S(1)}, u32[]{:S(2)}) copy-start(bf16[1024,128]{1,0:T(8,128)(2,1)S(1)} %get-tuple-element.183) | copy-start | bytes 786436
  95.8 35.7 %collective-permute-start = (bf16[4,2,128]{2,1,0:T(2,128)(2,1)S(1)}, bf16[4,2,128]{2,1,0:T(2,128)(2,1)S(1)}, u32[]{:S(2)}, u32[]{:S(2)}) collective-permute-start(bf16[4,2,128]{2,1,0:T(2,128)(2,1)S(1)} %slice.122), channel_id=1, source_target_pairs={{0,8},{8,16},{16,24},{1,9},{9,17},{17,25},{2,10},{10,18},{18,26},{... | collective-permute-start | bytes 6152 | tf_op jit(solution)/shard_map/ppermute | solution.py:105
  125.3 3.4 %copy-start.17 = (bf16[4,4,128,128]{3,2,1,0:T(8,128)(2,1)S(1)}, bf16[4,4,128,128]{3,2,1,0:T(8,128)(2,1)}, u32[]{:S(2)}) copy-start(bf16[4,4,128,128]{3,2,1,0:T(8,128)(2,1)} %get-tuple-element.75) | copy-start | bytes 1572868
  128.6 1.2 copy-start.15
  129.9 1.6 %copy-start.14 = (bf16[1024,128]{1,0:T(8,128)(2,1)S(1)}, bf16[1024,128]{1,0:T(8,128)(2,1)}, u32[]{:S(2)}) copy-start(bf16[1024,128]{1,0:T(8,128)(2,1)} %copy-done.13) | copy-start | bytes 786436
  129.9 1.7 %copy-start.16 = (bf16[1024,128]{1,0:T(8,128)(2,1)S(1)}, bf16[1024,128]{1,0:T(8,128)(2,1)}, u32[]{:S(2)}) copy-start(bf16[1024,128]{1,0:T(8,128)(2,1)} %get-tuple-element.180) | copy-start | bytes 786436
  131.9 3.4 %copy-start.1 = (bf16[8,2,128,2048]{3,2,1,0:T(8,128)(2,1)S(1)}, bf16[8,2,128,2048]{3,2,1,0:T(8,128)(2,1)}, u32[]{:S(2)}) copy-start(bf16[8,2,128,2048]{3,2,1,0:T(8,128)(2,1)} %get-tuple-element.77.wo_ref) | copy-start | bytes 25165828
